TPU v7x, 32 devices: a whole 2x2x4 slice. The times are simulated.
32 devices in a mesh: sp: 4 (over z), fs: 4 (over y, x), tp: 2 (over core).
Axes of the slice: x: 2, y: 2, z: 4, core: 2. Of those that a mesh axis runs over, the one named last changes fastest.
Arguments:
- inputs: bfloat16 [4, 512, 2048], P('fs', 'sp'), may hold values from -6 to 6
- input_norm_gain: bfloat16 [2048], replicated, may hold values from 0.099609375 to 1.8984375
- receptance_matrix: bfloat16 [2048, 1024], P('fs', 'tp'), may hold values from -0.125 to 0.125
- key_matrix: bfloat16 [2048, 1024], P('fs', 'tp'), may hold values from -0.125 to 0.125
- value_matrix: bfloat16 [2048, 1024], P('fs', 'tp'), may hold values from -0.125 to 0.125
- pooling_input_weight: bfloat16 [2048, 1024], P('fs', 'tp'), may hold values from -0.125 to 0.125
- decay_lower_matrix: bfloat16 [2048, 128], replicated, may hold values from -0.125 to 0.125
- decay_raise_matrix: bfloat16 [2, 64, 1024], P(None, None, 'tp'), may hold values from -1 to 1
- decay_offset_bias: float32 [2, 1024], P(None, 'tp'), may hold values from -13 to -3
- removal_lower_matrix: bfloat16 [2048, 128], replicated, may hold values from -0.125 to 0.125
- removal_raise_matrix: bfloat16 [2, 64, 1024], P(None, None, 'tp'), may hold values from -1 to 1
- removal_rate_bias: float32 [2, 1024], P(None, 'tp'), may hold values from -9 to 1.5
- tempo_scale: float32 [4, 2, 16, 512], P('fs', None, 'tp', 'sp'), may hold values from 0.3 to 3.2, as said below
- sudden_decay_extra: float32 [4, 2, 16, 512], P('fs', None, 'tp', 'sp'), may hold values from -2.8 to 0
- head_norm_gain: bfloat16 [1024], P('tp'), may hold values from 0.099609375 to 1.8984375
- group_mixing_weight: bfloat16 [4, 256, 256], P('tp'), may hold values from -0.375 to 0.375
- attention_output_matrix: bfloat16 [2048, 1024], P('fs', 'tp'), may hold values from -0.125 to 0.125
- pooling_output_matrix: bfloat16 [2048, 1024], P('fs', 'tp'), may hold values from -0.125 to 0.125
Outputs:
- mixed_out: bfloat16 [4, 512, 2048], P('fs', ('sp', 'tp'))
Inputs may be any that keep to these rules, and one draw needn't show every extreme that they name: `tempo_scale`: positive.
All inputs are finite; a program needn't handle non-finite values.
Results may differ from a plain program's by a relative error of at most 0.017.
Values may be sent and summed in bfloat16 or wider, within the bound.
A program may use at most 128 MiB of HBM per device.

v0:
```python
import functools

import jax
import jax.numpy as jnp
from jax import lax
from jax.experimental import pallas as pl
from jax.experimental.pallas import tpu as pltpu
from jax.sharding import PartitionSpec as P

HEAD = 64
GROUP_WIDTH = 256
LANES = 128
BLOCK = 16
HALO = 16

norm_eps = 1e-06
head_eps = 0.00064
unit_eps = 1e-06
f32 = jnp.float32
bf16 = jnp.bfloat16
VMEM = pl.BlockSpec(memory_space=pltpu.VMEM)


def dot(left, right):
    return jnp.dot(left.astype(bf16), right.astype(bf16), preferred_element_type=f32)


def dot_general(left, right, dims):
    return lax.dot_general(
        left.astype(bf16), right.astype(bf16), (dims, ((), ())), preferred_element_type=f32
    )


def dot_rows(left, right):
    return dot_general(left, right, ((1,), (1,)))


def dot_cols(left, right):
    return dot_general(left, right, ((0,), (0,)))


def exact_dot(left, right, dims):
    return lax.dot_general(
        left, right, (dims, ((), ())), preferred_element_type=f32, precision=lax.Precision.HIGHEST
    )


def remote(src, dst, send, recv, axis, peer):
    return pltpu.make_async_remote_copy(
        src_ref=src,
        dst_ref=dst,
        send_sem=send,
        recv_sem=recv,
        device_id={axis: peer},
        device_id_type=pl.DeviceIdType.MESH,
    )


def greet(barrier, axis, peer):
    pl.semaphore_signal(
        barrier, inc=1, device_id={axis: peer}, device_id_type=pl.DeviceIdType.MESH
    )


def front_kernel(
    n,
    x_ref,
    gain_ref,
    wr_ref,
    wk_ref,
    wv_ref,
    wp_ref,
    dl_ref,
    rl_ref,
    out_ref,
    lat_ref,
    mine,
    cells,
    part,
    landed,
    xs,
    xr,
    ps,
    pr,
):
    me = lax.axis_index("fs")
    barrier = pltpu.get_barrier_semaphore()
    for d in range(1, n):
        greet(barrier, "fs", lax.rem(me + d, n))
    width = wr_ref.shape[0]
    x = x_ref[0].astype(f32)
    normed = (
        x
        * lax.rsqrt(jnp.mean(x * x, axis=-1, keepdims=True) + norm_eps)
        * gain_ref[...].astype(f32)
    ).astype(bf16)
    for j in range(n):
        mine[j] = normed[:, j * width : (j + 1) * width]
    pl.semaphore_wait(barrier, n - 1)
    order = [n // 2] + [d for d in range(1, n) if d != n // 2]
    moves = []
    for d in order:
        peer = lax.rem(me + d, n)
        copy = remote(mine.at[peer], cells.at[me], xs.at[d], xr.at[d], "fs", peer)
        copy.start()
        moves.append(copy)
    decay = jnp.zeros((x.shape[0], dl_ref.shape[1]), f32)
    rate = jnp.zeros((x.shape[0], rl_ref.shape[1]), f32)
    for j in range(n):
        block = mine[j]
        decay = decay + dot(block, dl_ref[j * width : (j + 1) * width])
        rate = rate + dot(block, rl_ref[j * width : (j + 1) * width])
    lat_ref[0] = jnp.tanh(decay.astype(bf16).astype(f32)).astype(bf16)
    lat_ref[1] = rate.astype(bf16)
    weights = (wk_ref, wr_ref, wv_ref, wp_ref)
    copies = []
    for copy, d in zip(moves, order):
        copy.wait_recv()
    for m, weight in enumerate(weights):
        for d in order:
            peer = lax.rem(me + d, n)
            part[peer, m] = dot(cells[peer], weight[...]).astype(bf16)
            copy = remote(
                part.at[peer, m], landed.at[me, m], ps.at[d, m], pr.at[d, m], "fs", peer
            )
            copy.start()
            copies.append((m, copy))
    for m, weight in enumerate(weights):
        total = dot(mine[me], weight[...])
        for at, copy in copies:
            if at == m:
                copy.wait_recv()
        for d in range(1, n):
            total = total + landed[lax.rem(me + d, n), m].astype(f32)
        out_ref[m] = total.astype(bf16)
    for copy in moves:
        copy.wait_send()
    for _, copy in copies:
        copy.wait_send()


def mixer_kernel(
    p4_ref,
    lat_ref,
    draise_ref,
    dbias_ref,
    rraise_ref,
    rbias_ref,
    tempo_ref,
    extra_ref,
    query_ref,
    local_ref,
    transfer_ref,
    carried_ref,
):
    pair = pl.program_id(0)
    tokens = p4_ref.shape[1]
    kf = p4_ref[0].astype(f32)
    rf = p4_ref[1].astype(f32)
    value = p4_ref[2]
    lane = lax.broadcasted_iota(jnp.int32, (tokens, LANES), 1)
    row = lax.broadcasted_iota(jnp.int32, (tokens, LANES), 0)
    head0 = lane < HEAD
    k2 = kf * kf
    s0 = jnp.sum(jnp.where(head0, k2, 0.0), axis=-1, keepdims=True)
    s1 = jnp.sum(jnp.where(head0, 0.0, k2), axis=-1, keepdims=True)
    unit = kf * lax.rsqrt(jnp.where(head0, s0, s1) + unit_eps)
    heads = tempo_ref.shape[1]
    spread = (
        lax.broadcasted_iota(jnp.int32, (heads, LANES), 0)
        == 2 * pair + lax.broadcasted_iota(jnp.int32, (heads, LANES), 1) // HEAD
    ).astype(f32)
    blocks = tokens // BLOCK
    zero_row = jnp.zeros((1, LANES), f32)
    eye = (row == lane).astype(f32)
    sizes = []
    size = 1
    while size < tokens:
        sizes.append(size)
        size *= 2

    def level_mask(k):
        return ((row >> (k + 1)) == (lane >> (k + 1))) & ((row >> k) != (lane >> k))

    ways = []
    for d in range(2):
        lat_mask = head0 if d == 0 else ~head0
        lat_d = jnp.where(lat_mask, lat_ref[0].astype(f32), 0.0)
        lat_r = jnp.where(lat_mask, lat_ref[1].astype(f32), 0.0)
        pre = dbias_ref[d : d + 1] + dot(lat_d, draise_ref[...])
        velocity = jax.nn.sigmoid(pre) * 0.6065306597126334
        tempo = exact_dot(tempo_ref[d], spread, ((0,), (0,)))
        extra = exact_dot(extra_ref[d], spread, ((0,), (0,)))
        ld = -velocity * tempo + extra
        rate = jax.nn.sigmoid(rbias_ref[d : d + 1] + dot(lat_r, rraise_ref[...]))
        removal = unit * rate
        written = kf * rate
        upto = (lane <= row) if d == 0 else (lane >= row)
        inner = exact_dot(upto.astype(f32), ld, ((1,), (0,)))
        excl = inner - ld
        grams = []
        for i in range(blocks):
            lo, hi = i * BLOCK, (i + 1) * BLOCK
            if d == 0:
                base = inner[lo - 1 : lo] if i > 0 else zero_row
            else:
                base = inner[hi : hi + 1] if i < blocks - 1 else zero_row
            ahead = unit[lo:hi] * jnp.exp(excl[lo:hi] - base)
            query = rf[lo:hi] * jnp.exp(inner[lo:hi] - base)
            grow = jnp.exp(jnp.minimum(base - inner, 80.0))
            right = jnp.concatenate([(removal * grow).astype(bf16), (written * grow).astype(bf16)], 0)
            h0 = head0[lo:hi]
            left = jnp.concatenate(
                [
                    jnp.where(h0, ahead, 0.0),
                    jnp.where(h0, 0.0, ahead),
                    jnp.where(h0, query, 0.0),
                    jnp.where(h0, 0.0, query),
                ],
                0,
            )
            grams.append(dot_rows(left, right))
        strict = (lane < row) if d == 0 else (lane > row)

        def gathered(place, at, mask):
            rows = jnp.concatenate(
                [g[place * BLOCK : (place + 1) * BLOCK, at * tokens : (at + 1) * tokens] for g in grams],
                0,
            )
            return jnp.where(mask, rows, 0.0)

        way = dict(inner=inner, excl=excl, removal=removal, written=written)
        way["link"] = [gathered(h, 0, strict) for h in range(2)]
        way["link_write"] = [gathered(h, 1, strict).astype(bf16) for h in range(2)]
        way["read"] = [gathered(2 + h, 0, upto).astype(bf16) for h in range(2)]
        way["read_write"] = [gathered(2 + h, 1, upto).astype(bf16) for h in range(2)]
        ways.append(way)

    links = [way["link"][h] for way in ways for h in range(2)]
    inverses = [eye - jnp.where(level_mask(0), a, 0.0) for a in links]
    for k in range(1, len(sizes)):
        mask = level_mask(k)
        firsts = [dot(t, jnp.where(mask, a, 0.0)) for t, a in zip(inverses, links)]
        inverses = [t - dot(u, t) for t, u in zip(inverses, firsts)]

    block_diag = (row < HEAD) == head0
    local = jnp.zeros((tokens, LANES), f32)
    for d, way in enumerate(ways):
        inner, excl = way["inner"], way["excl"]
        last = inner[tokens - 1 : tokens] if d == 0 else inner[0:1]
        ahead = unit * jnp.exp(excl)
        query = rf * jnp.exp(inner)
        tail = jnp.exp(last - inner)

        def chosen(pieces):
            return jnp.where(head0, pieces[0], pieces[1])

        base = chosen([dot(way["link_write"][h], value) for h in range(2)])
        rhs = jnp.concatenate([ahead.astype(bf16), base.astype(bf16)], 1)
        solved = [dot(inverses[2 * d + h], rhs) for h in range(2)]
        pull_map = -chosen([s[:, :LANES] for s in solved])
        pull_base = -chosen([s[:, LANES:] for s in solved])
        remove_tail = (way["removal"] * tail).astype(bf16)
        write_tail = (way["written"] * tail).astype(bf16)
        both = jnp.concatenate([pull_map.astype(bf16), pull_base.astype(bf16)], 1)
        seen = [dot(way["read"][h], both) for h in range(2)]
        query_ref[d] = (query + chosen([s[:, :LANES] for s in seen])).astype(bf16)
        local = (
            local
            + chosen([s[:, LANES:] for s in seen])
            + chosen([dot(way["read_write"][h], value) for h in range(2)])
        )
        transfer = jnp.where(block_diag, dot_cols(pull_map, remove_tail), 0.0) + eye * jnp.exp(last)
        transfer_ref[d, 0] = transfer
        carried = dot_cols(
            jnp.concatenate([pull_base.astype(bf16), value], 0),
            jnp.concatenate([remove_tail, write_tail], 0),
        )
        carried = jnp.where(block_diag, carried, 0.0)
        carried_ref[d, 0] = carried[:HEAD] + carried[HEAD:]
    local_ref[...] = local


def tail_kernel(
    nsp,
    nfs,
    ntp,
    query_ref,
    local_ref,
    transfer_ref,
    carried_ref,
    p4_ref,
    mix_ref,
    gain_ref,
    wa_ref,
    wp_ref,
    out_ref,
    edge,
    halo,
    incoming,
    leaving,
    act,
    tsend,
    trecv,
    osend,
    orecv,
    hs,
    hr,
    ss,
    sr,
    gs,
    gr,
    ts,
    tr,
    os,
    orr,
):
    z = lax.axis_index("sp")
    me = lax.axis_index("fs")
    core = lax.axis_index("tp")
    tokens, channels = local_ref.shape
    pairs = transfer_ref.shape[1]
    half_rows = tokens // ntp
    has_prev = z > 0
    has_next = z < nsp - 1
    prev = jnp.maximum(z - 1, 0)
    after = jnp.minimum(z + 1, nsp - 1)

    barrier = pltpu.get_barrier_semaphore()
    for d in range(1, nfs):
        greet(barrier, "fs", lax.rem(me + d, nfs))
    for d in range(1, ntp):
        greet(barrier, "tp", lax.rem(core + d, ntp))
    pl.when(has_prev)(lambda: greet(barrier, "sp", prev))
    pl.when(has_next)(lambda: greet(barrier, "sp", after))
    count = nfs + ntp - 2 + jnp.where(has_prev, 1, 0) + jnp.where(has_next, 1, 0)
    edge[0] = p4_ref[3, :HALO]
    edge[1] = p4_ref[3, tokens - HALO :]
    pl.semaphore_wait(barrier, count)

    sides = [(has_prev, prev, has_next), (has_next, after, has_prev)]
    state_copies = [
        remote(leaving.at[0], incoming.at[0], ss.at[0], sr.at[0], "sp", after),
        remote(leaving.at[1], incoming.at[1], ss.at[1], sr.at[1], "sp", prev),
    ]
    halo_copies = [
        remote(edge.at[1], halo.at[0], hs.at[0], hr.at[0], "sp", after),
        remote(edge.at[0], halo.at[1], hs.at[1], hr.at[1], "sp", prev),
    ]
    sends = [has_next, has_prev]
    takes = [has_prev, has_next]

    def relay(d):
        @pl.when(takes[d])
        def _():
            state_copies[d].wait_recv()

        @pl.when(jnp.logical_not(takes[d]))
        def _():
            incoming[d] = jnp.zeros_like(incoming[d])

        @pl.when(sends[d])
        def _():
            for p in range(pairs):
                rows = slice(p * HEAD, (p + 1) * HEAD)
                leaving[d, rows] = (
                    dot(incoming[d, rows], transfer_ref[d, p]) + carried_ref[d, p]
                ).astype(bf16)
            state_copies[d].start()

    def start_halo(d):
        pl.when(sends[d])(lambda: halo_copies[d].start())

    early = 2 * z < nsp

    @pl.when(early)
    def _():
        relay(0)

    @pl.when(jnp.logical_not(early))
    def _():
        relay(1)

    for d in range(2):
        start_halo(d)
    for d in range(2):

        @pl.when(takes[d])
        def _():
            halo_copies[d].wait_recv()

        @pl.when(jnp.logical_not(takes[d]))
        def _():
            halo[d] = jnp.zeros_like(halo[d])

    span = tokens + 2 * HALO
    rim = jnp.concatenate([halo[0], p4_ref[3], halo[1]], 0)
    here = lax.broadcasted_iota(jnp.int32, (tokens, span), 0)
    there = lax.broadcasted_iota(jnp.int32, (tokens, span), 1) - HALO
    position = z * tokens + lax.broadcasted_iota(jnp.int32, (tokens, GROUP_WIDTH), 0)
    length = tokens * nsp
    groups_here = channels // GROUP_WIDTH
    for member in range(groups_here):
        cols = slice(member * GROUP_WIDTH, (member + 1) * GROUP_WIDTH)
        reach = jnp.left_shift(1, core * groups_here + member)
        window = jnp.where((there >= here - reach) & (there < here + reach), 1.0, 0.0)
        total = dot(window, rim[:, cols])
        size = (
            jnp.minimum(position + reach, length) - jnp.maximum(position - reach, 0)
        ).astype(f32)
        diff = (total / size - p4_ref[3, :, cols].astype(f32)).astype(bf16)
        act[me, 0, :, cols] = dot(diff, mix_ref[member]).astype(bf16)
    order = [nfs // 2] + [d for d in range(1, nfs) if d != nfs // 2]
    shares = []
    for d in order:
        peer = lax.rem(me + d, nfs)
        copy = remote(act.at[me, 0], act.at[me, 0], gs.at[d, 0], gr.at[d, 0], "fs", peer)
        copy.start()
        shares.append(copy)

    @pl.when(early)
    def _():
        relay(1)

    @pl.when(jnp.logical_not(early))
    def _():
        relay(0)

    head0 = lax.broadcasted_iota(jnp.int32, (tokens, LANES), 1) < HEAD
    top0 = lax.broadcasted_iota(jnp.int32, (HEAD, LANES), 1) < HEAD
    for p in range(pairs):
        lanes = slice(p * LANES, (p + 1) * LANES)
        readout = local_ref[:, lanes]
        for d in range(2):
            state = incoming[d, p * HEAD : (p + 1) * HEAD].astype(f32)
            wide = jnp.concatenate(
                [jnp.where(top0, state, 0.0), jnp.where(top0, 0.0, state)], 0
            )
            readout = readout + dot_rows(query_ref[d, :, lanes], wide)

        def head_mean(cells):
            low = jnp.sum(jnp.where(head0, cells, 0.0), axis=-1, keepdims=True)
            high = jnp.sum(jnp.where(head0, 0.0, cells), axis=-1, keepdims=True)
            return jnp.where(head0, low, high) * (1.0 / HEAD)

        centred = readout - head_mean(readout)
        scaled = centred * lax.rsqrt(head_mean(centred * centred) + head_eps)
        act[me, 1, :, lanes] = (scaled * gain_ref[:, lanes].astype(f32)).astype(bf16)
    for d in order:
        peer = lax.rem(me + d, nfs)
        copy = remote(act.at[me, 1], act.at[me, 1], gs.at[d, 1], gr.at[d, 1], "fs", peer)
        copy.start()
        shares.append(copy)

    other = lax.rem(core + 1, ntp)
    mine_at = pl.multiple_of(core * half_rows, half_rows)
    other_at = pl.multiple_of(other * half_rows, half_rows)

    def product(seq, rows):
        return dot_rows(act[seq, 1, rows], wa_ref[...]) + dot_rows(act[seq, 0, rows], wp_ref[...])

    returns = []
    swaps = []
    turns = [0] + [d for d in range(1, nfs) if d != nfs // 2] + [nfs // 2]
    for d in turns:
        seq = lax.rem(me + nfs - d, nfs)
        if d:
            for copy, at in zip(shares, order + order):
                if at == d:
                    copy.wait_recv()
        tsend[d] = product(seq, pl.ds(other_at, half_rows)).astype(bf16)
        swap = remote(tsend.at[d], trecv.at[d], ts.at[d], tr.at[d], "tp", other)
        swap.start()
        swaps.append(swap)
        kept = product(seq, pl.ds(mine_at, half_rows))
        swap.wait_recv()
        whole = (kept + trecv[d].astype(f32)).astype(bf16)
        if d:
            osend[d] = whole
            copy = remote(osend.at[d], orecv.at[me], os.at[d], orr.at[d], "fs", seq)
            copy.start()
            returns.append(copy)
        else:
            orecv[me] = whole
    for copy in returns:
        copy.wait_recv()
    for j in range(nfs):
        out_ref[0, :, j * channels : (j + 1) * channels] = orecv[j]
    for copy in shares + swaps + returns:
        copy.wait_send()
    for d in range(2):

        @pl.when(sends[d])
        def _():
            state_copies[d].wait_send()
            halo_copies[d].wait_send()


def shards(
    inputs,
    input_norm_gain,
    receptance_matrix,
    key_matrix,
    value_matrix,
    pooling_input_weight,
    decay_lower_matrix,
    decay_raise_matrix,
    decay_offset_bias,
    removal_lower_matrix,
    removal_raise_matrix,
    removal_rate_bias,
    tempo_scale,
    sudden_decay_extra,
    head_norm_gain,
    group_mixing_weight,
    attention_output_matrix,
    pooling_output_matrix,
):
    nsp, nfs, ntp = lax.axis_size("sp"), lax.axis_size("fs"), lax.axis_size("tp")
    _, tokens, features = inputs.shape
    depth, channels = key_matrix.shape
    pairs = channels // LANES
    heads = channels // HEAD
    dma = pltpu.SemaphoreType.DMA
    limit = 60 * 1024 * 1024
    p4, lat = pl.pallas_call(
        functools.partial(front_kernel, nfs),
        out_shape=(
            jax.ShapeDtypeStruct((4, tokens, channels), bf16),
            jax.ShapeDtypeStruct((2, tokens, decay_lower_matrix.shape[1]), bf16),
        ),
        in_specs=[VMEM] * 8,
        out_specs=(VMEM, VMEM),
        scratch_shapes=[
            pltpu.VMEM((nfs, tokens, depth), bf16),
            pltpu.VMEM((nfs, tokens, depth), bf16),
            pltpu.VMEM((nfs, 4, tokens, channels), bf16),
            pltpu.VMEM((nfs, 4, tokens, channels), bf16),
            dma((nfs,)),
            dma((nfs,)),
            dma((nfs, 4)),
            dma((nfs, 4)),
        ],
        compiler_params=pltpu.CompilerParams(
            collective_id=0, has_side_effects=True, vmem_limit_bytes=limit
        ),
        name="front",
    )(
        inputs,
        input_norm_gain[None],
        receptance_matrix,
        key_matrix,
        value_matrix,
        pooling_input_weight,
        decay_lower_matrix,
        removal_lower_matrix,
    )

    def whole(*shape):
        return pl.BlockSpec(shape, lambda p: (0,) * len(shape))

    rank2 = decay_raise_matrix.shape[0] * decay_raise_matrix.shape[1]
    query, local, transfer, carried = pl.pallas_call(
        mixer_kernel,
        grid=(pairs,),
        out_shape=(
            jax.ShapeDtypeStruct((2, tokens, channels), bf16),
            jax.ShapeDtypeStruct((tokens, channels), f32),
            jax.ShapeDtypeStruct((2, pairs, LANES, LANES), f32),
            jax.ShapeDtypeStruct((2, pairs, HEAD, LANES), f32),
        ),
        in_specs=[
            pl.BlockSpec((4, tokens, LANES), lambda p: (0, 0, p)),
            whole(2, tokens, decay_lower_matrix.shape[1]),
            pl.BlockSpec((rank2, LANES), lambda p: (0, p)),
            pl.BlockSpec((2, LANES), lambda p: (0, p)),
            pl.BlockSpec((rank2, LANES), lambda p: (0, p)),
            pl.BlockSpec((2, LANES), lambda p: (0, p)),
            whole(2, heads, tokens),
            whole(2, heads, tokens),
        ],
        out_specs=(
            pl.BlockSpec((2, tokens, LANES), lambda p: (0, 0, p)),
            pl.BlockSpec((tokens, LANES), lambda p: (0, p)),
            pl.BlockSpec((2, 1, LANES, LANES), lambda p: (0, p, 0, 0)),
            pl.BlockSpec((2, 1, HEAD, LANES), lambda p: (0, p, 0, 0)),
        ),
        compiler_params=pltpu.CompilerParams(
            vmem_limit_bytes=limit, dimension_semantics=("arbitrary",)
        ),
        name="mixer",
    )(
        p4,
        lat,
        decay_raise_matrix.reshape(rank2, channels),
        decay_offset_bias,
        removal_raise_matrix.reshape(rank2, channels),
        removal_rate_bias,
        tempo_scale[0],
        sudden_decay_extra[0],
    )
    return pl.pallas_call(
        functools.partial(tail_kernel, nsp, nfs, ntp),
        out_shape=jax.ShapeDtypeStruct((1, tokens // ntp, features), bf16),
        in_specs=[VMEM] * 9,
        out_specs=VMEM,
        scratch_shapes=[
            pltpu.VMEM((2, HALO, channels), bf16),
            pltpu.VMEM((2, HALO, channels), bf16),
            pltpu.VMEM((2, pairs * HEAD, LANES), bf16),
            pltpu.VMEM((2, pairs * HEAD, LANES), bf16),
            pltpu.VMEM((nfs, 2, tokens, channels), bf16),
            pltpu.VMEM((nfs, tokens // ntp, depth), bf16),
            pltpu.VMEM((nfs, tokens // ntp, depth), bf16),
            pltpu.VMEM((nfs, tokens // ntp, depth), bf16),
            pltpu.VMEM((nfs, tokens // ntp, depth), bf16),
            dma((2,)),
            dma((2,)),
            dma((2,)),
            dma((2,)),
            dma((nfs, 2)),
            dma((nfs, 2)),
            dma((nfs,)),
            dma((nfs,)),
            dma((nfs,)),
            dma((nfs,)),
        ],
        compiler_params=pltpu.CompilerParams(
            collective_id=1, has_side_effects=True, vmem_limit_bytes=limit
        ),
        name="tail",
    )(
        query,
        local,
        transfer,
        carried,
        p4,
        group_mixing_weight,
        head_norm_gain[None],
        attention_output_matrix,
        pooling_output_matrix,
    )


def solution(mesh):
    in_specs = (
        P("fs", "sp", None),
        P(),
        P("fs", "tp"),
        P("fs", "tp"),
        P("fs", "tp"),
        P("fs", "tp"),
        P(),
        P(None, None, "tp"),
        P(None, "tp"),
        P(),
        P(None, None, "tp"),
        P(None, "tp"),
        P("fs", None, "tp", "sp"),
        P("fs", None, "tp", "sp"),
        P("tp"),
        P("tp", None, None),
        P("fs", "tp"),
        P("fs", "tp"),
    )
    out_specs = P("fs", ("sp", "tp"), None)
    return jax.shard_map(shards, mesh=mesh, in_specs=in_specs, out_specs=out_specs, check_vma=False)
```

profile of v0, /device:TPU:0, one launch (start us, length us, event | category | flops | bytes accessed | tf_op | source)
XLA Modules:
  0.0 90.2 jit_solution(6771113022569808825)
XLA Ops:
  0.0 0.0 copy-start
  0.0 0.0 copy-start.1
  0.0 0.7 copy-done.1
  0.7 0.6 broadcast_in_dim.7.gain_ref
  1.3 0.0 copy-done
  1.3 0.6 broadcast_in_dim.6.gain_ref
  1.9 39.0 %front.1 = (bf16[4,128,512]{2,1,0:T(8,128)(2,1)}, bf16[2,128,128]{2,1,0:T(8,128)(2,1)}) custom-call(bf16[1,128,2048]{2,1,0:T(8,128)(2,1)} %x_ref.1, bf16[1,2048]{1,0:T(2,128)(2,1)} %broadcast_in_dim.6.gain_ref, bf16[512,512]{1,0:T(8,128)(2,1)} %wr_ref.1, bf16[512,512]{1,0:T(8,128)(2,1)} %wk_ref.1, bf16[512,512]{1,0:T(8,128)(2,1)} %wv_ref.1, ...), custom_call_target="tpu_custom_call" | custom-call | tf_op jit(solution)/shard_map/front/pallas_call | solution.py:526
  40.9 17.2 %mixer.1 = (bf16[2,128,512]{2,1,0:T(8,128)(2,1)}, f32[128,512]{1,0:T(8,128)}, f32[2,4,128,128]{3,2,1,0:T(8,128)}, f32[2,4,64,128]{3,2,1,0:T(8,128)}) custom-call(bf16[4,128,512]{2,1,0:T(8,128)(2,1)} %get-tuple-element.11.p4_ref, bf16[2,128,128]{2,1,0:T(8,128)(2,1)} %get-tuple-element.12.lat_ref, bf16[128,512]{1,0:T(8,128)(2,1)} %bitcast.4, ...), custom_call_target="tpu_custom_call" | custom-call | tf_op jit(solution)/shard_map/mixer/pallas_call | solution.py:563
  58.1 30.4 %tail.1 = bf16[1,64,2048]{2,1,0:T(8,128)(2,1)} custom-call(bf16[2,128,512]{2,1,0:T(8,128)(2,1)} %get-tuple-element.13.query_ref, f32[128,512]{1,0:T(8,128)} %get-tuple-element.14.local_ref, f32[2,4,128,128]{3,2,1,0:T(8,128)} %get-tuple-element.15.transfer_ref, f32[2,4,64,128]{3,2,1,0:T(8,128)} %get-tuple-element.16.carried_ref, ...), custom_call_target="tpu_custom_call" | custom-call | tf_op jit(solution)/shard_map/tail/pallas_call | solution.py:602
  88.5 1.7 %copy.20 = bf16[1,64,2048]{2,1,0:T(8,128)(2,1)} copy(bf16[1,64,2048]{2,1,0:T(8,128)(2,1)} %tail.1) | data formatting | bytes 524288
Async XLA Ops:
  0.0 1.3 %copy-start = (bf16[2048]{0:T(1024)(128)(2,1)S(1)}, bf16[2048]{0:T(1024)(128)(2,1)}, u32[]{:S(2)}) copy-start(bf16[2048]{0:T(1024)(128)(2,1)} %param.19) | copy-start | bytes 12292
  0.0 0.7 copy-start.1
where the time goes:
time: 90.4 us; the launch traced here: 90.2 us
  Pallas kernels  86.6 us (96%)
  local copies, waits for them, and re-layouts  3.57 us (4%)
    pallas_call x1, Pallas kernels, shards(): pl.pallas_call(functools.partial(front_kernel, nfs), out_shape=(jax.Shape...  39 us
    pallas_call x1, Pallas kernels, shards(): pl.pallas_call(functools.partial(tail_kernel, nsp, nfs, ntp), out_shape=j...  30.4 us
    pallas_call x1, Pallas kernels, shards(): pl.pallas_call(mixer_kernel, grid=(pairs,), out_shape=(jax.ShapeDtypeStru...  17.2 us
    unnamed x5, local copies, waits for them, and re-layouts  2.37 us

commit v1 on v0

--- a/solution.py
+++ b/solution.py
@@ -62,32 +62,31 @@
     )
 
 
-def front_kernel(
+def front_part(
     n,
     x_ref,
     gain_ref,
-    wr_ref,
-    wk_ref,
-    wv_ref,
-    wp_ref,
-    dl_ref,
-    rl_ref,
-    out_ref,
+    weights,
+    lowers,
+    loads,
+    pool_ref,
     lat_ref,
     mine,
     cells,
     part,
+    pool_part,
     landed,
+    pool_landed,
     xs,
     xr,
     ps,
     pr,
+    count,
+    mix_pair,
 ):
     me = lax.axis_index("fs")
-    barrier = pltpu.get_barrier_semaphore()
-    for d in range(1, n):
-        greet(barrier, "fs", lax.rem(me + d, n))
-    width = wr_ref.shape[0]
+    width = x_ref.shape[2] // n
+    pairs = part.shape[1]
     x = x_ref[0].astype(f32)
     normed = (
         x
@@ -96,7 +95,7 @@
     ).astype(bf16)
     for j in range(n):
         mine[j] = normed[:, j * width : (j + 1) * width]
-    pl.semaphore_wait(barrier, n - 1)
+    pl.semaphore_wait(pltpu.get_barrier_semaphore(), count)
     order = [n // 2] + [d for d in range(1, n) if d != n // 2]
     moves = []
     for d in order:
@@ -104,6 +103,9 @@
         copy = remote(mine.at[peer], cells.at[me], xs.at[d], xr.at[d], "fs", peer)
         copy.start()
         moves.append(copy)
+    for load in loads:
+        load.wait()
+    dl_ref, rl_ref = lowers
     decay = jnp.zeros((x.shape[0], dl_ref.shape[1]), f32)
     rate = jnp.zeros((x.shape[0], rl_ref.shape[1]), f32)
     for j in range(n):
@@ -112,35 +114,71 @@
         rate = rate + dot(block, rl_ref[j * width : (j + 1) * width])
     lat_ref[0] = jnp.tanh(decay.astype(bf16).astype(f32)).astype(bf16)
     lat_ref[1] = rate.astype(bf16)
-    weights = (wk_ref, wr_ref, wv_ref, wp_ref)
-    copies = []
-    for copy, d in zip(moves, order):
+    for copy in moves:
         copy.wait_recv()
-    for m, weight in enumerate(weights):
+
+    def pair_copy(d, p):
+        peer = lax.rem(me + d, n)
+        return remote(
+            part.at[peer, p], landed.at[me, p], ps.at[d, p], pr.at[d, p], "fs", peer
+        )
+
+    def pool_copy(d):
+        peer = lax.rem(me + d, n)
+        return remote(
+            pool_part.at[peer],
+            pool_landed.at[me],
+            ps.at[d, pairs],
+            pr.at[d, pairs],
+            "fs",
+            peer,
+        )
+
+    for p in range(pairs):
         for d in order:
             peer = lax.rem(me + d, n)
-            part[peer, m] = dot(cells[peer], weight[...]).astype(bf16)
-            copy = remote(
-                part.at[peer, m], landed.at[me, m], ps.at[d, m], pr.at[d, m], "fs", peer
-            )
-            copy.start()
-            copies.append((m, copy))
-    for m, weight in enumerate(weights):
-        total = dot(mine[me], weight[...])
-        for at, copy in copies:
-            if at == m:
-                copy.wait_recv()
+            for m in range(3):
+                part[peer, p, m] = dot(
+                    cells[peer], weights[m][:, p * LANES : (p + 1) * LANES]
+                ).astype(bf16)
+            pair_copy(d, p).start()
+    for d in order:
+        peer = lax.rem(me + d, n)
+        pool_part[peer] = dot(cells[peer], weights[3][...]).astype(bf16)
+        pool_copy(d).start()
+
+    def pair_step(p, carry):
+        lanes = pl.ds(pl.multiple_of(p * LANES, LANES), LANES)
+        owned = [dot(mine[me], weights[m][:, lanes]) for m in range(3)]
         for d in range(1, n):
-            total = total + landed[lax.rem(me + d, n), m].astype(f32)
-        out_ref[m] = total.astype(bf16)
+            pair_copy(d, p).wait_recv()
+        for d in range(1, n):
+            peer = lax.rem(me + d, n)
+            owned = [o + landed[peer, p, m].astype(f32) for m, o in enumerate(owned)]
+        mix_pair(p, lanes, *[o.astype(bf16) for o in owned])
+        return carry
+
+    lax.fori_loop(0, pairs, pair_step, 0)
+    total = dot(mine[me], weights[3][...])
+    for d in range(1, n):
+        pool_copy(d).wait_recv()
+    for d in range(1, n):
+        total = total + pool_landed[lax.rem(me + d, n)].astype(f32)
+    pool_ref[...] = total.astype(bf16)
     for copy in moves:
         copy.wait_send()
-    for _, copy in copies:
-        copy.wait_send()
-
-
-def mixer_kernel(
-    p4_ref,
+    for d in range(1, n):
+        for p in range(pairs):
+            pair_copy(d, p).wait_send()
+        pool_copy(d).wait_send()
+
+
+def mix_pair(
+    pair,
+    lanes,
+    key,
+    receptance,
+    value,
     lat_ref,
     draise_ref,
     dbias_ref,
@@ -153,11 +191,9 @@
     transfer_ref,
     carried_ref,
 ):
-    pair = pl.program_id(0)
-    tokens = p4_ref.shape[1]
-    kf = p4_ref[0].astype(f32)
-    rf = p4_ref[1].astype(f32)
-    value = p4_ref[2]
+    tokens = key.shape[0]
+    kf = key.astype(f32)
+    rf = receptance.astype(f32)
     lane = lax.broadcasted_iota(jnp.int32, (tokens, LANES), 1)
     row = lax.broadcasted_iota(jnp.int32, (tokens, LANES), 0)
     head0 = lane < HEAD
@@ -187,12 +223,12 @@
         lat_mask = head0 if d == 0 else ~head0
         lat_d = jnp.where(lat_mask, lat_ref[0].astype(f32), 0.0)
         lat_r = jnp.where(lat_mask, lat_ref[1].astype(f32), 0.0)
-        pre = dbias_ref[d : d + 1] + dot(lat_d, draise_ref[...])
+        pre = dbias_ref[d : d + 1, lanes] + dot(lat_d, draise_ref[:, lanes])
         velocity = jax.nn.sigmoid(pre) * 0.6065306597126334
         tempo = exact_dot(tempo_ref[d], spread, ((0,), (0,)))
         extra = exact_dot(extra_ref[d], spread, ((0,), (0,)))
         ld = -velocity * tempo + extra
-        rate = jax.nn.sigmoid(rbias_ref[d : d + 1] + dot(lat_r, rraise_ref[...]))
+        rate = jax.nn.sigmoid(rbias_ref[d : d + 1, lanes] + dot(lat_r, rraise_ref[:, lanes]))
         removal = unit * rate
         written = kf * rate
         upto = (lane <= row) if d == 0 else (lane >= row)
@@ -264,37 +300,72 @@
         write_tail = (way["written"] * tail).astype(bf16)
         both = jnp.concatenate([pull_map.astype(bf16), pull_base.astype(bf16)], 1)
         seen = [dot(way["read"][h], both) for h in range(2)]
-        query_ref[d] = (query + chosen([s[:, :LANES] for s in seen])).astype(bf16)
+        query_ref[d, :, lanes] = (query + chosen([s[:, :LANES] for s in seen])).astype(bf16)
         local = (
             local
             + chosen([s[:, LANES:] for s in seen])
             + chosen([dot(way["read_write"][h], value) for h in range(2)])
         )
         transfer = jnp.where(block_diag, dot_cols(pull_map, remove_tail), 0.0) + eye * jnp.exp(last)
-        transfer_ref[d, 0] = transfer
+        transfer_ref[d, pair] = transfer
         carried = dot_cols(
             jnp.concatenate([pull_base.astype(bf16), value], 0),
             jnp.concatenate([remove_tail, write_tail], 0),
         )
         carried = jnp.where(block_diag, carried, 0.0)
-        carried_ref[d, 0] = carried[:HEAD] + carried[HEAD:]
-    local_ref[...] = local
-
-
-def tail_kernel(
+        carried_ref[d, pair] = carried[:HEAD] + carried[HEAD:]
+    local_ref[:, lanes] = local
+
+
+def layer_kernel(
     nsp,
     nfs,
     ntp,
+    x_ref,
+    in_gain_ref,
+    wk_hbm,
+    wr_hbm,
+    wv_hbm,
+    wi_hbm,
+    dl_hbm,
+    rl_hbm,
+    draise_ref,
+    dbias_ref,
+    rraise_ref,
+    rbias_ref,
+    tempo_ref,
+    extra_ref,
+    mix_hbm,
+    gain_ref,
+    wa_hbm,
+    wp_hbm,
+    out_ref,
+    wk_ref,
+    wr_ref,
+    wv_ref,
+    wi_ref,
+    dl_ref,
+    rl_ref,
+    mix_ref,
+    wa_ref,
+    wp_ref,
+    loaded,
+    mine,
+    cells,
+    part,
+    pool_part,
+    landed,
+    pool_landed,
+    xs,
+    xr,
+    ps,
+    pr,
+    lat_ref,
+    pool_ref,
     query_ref,
     local_ref,
     transfer_ref,
     carried_ref,
-    p4_ref,
-    mix_ref,
-    gain_ref,
-    wa_ref,
-    wp_ref,
-    out_ref,
     edge,
     halo,
     incoming,
@@ -334,15 +405,69 @@
     pl.when(has_prev)(lambda: greet(barrier, "sp", prev))
     pl.when(has_next)(lambda: greet(barrier, "sp", after))
     count = nfs + ntp - 2 + jnp.where(has_prev, 1, 0) + jnp.where(has_next, 1, 0)
-    edge[0] = p4_ref[3, :HALO]
-    edge[1] = p4_ref[3, tokens - HALO :]
-    pl.semaphore_wait(barrier, count)
+    sources = (dl_hbm, rl_hbm, wk_hbm, wr_hbm, wv_hbm, wi_hbm, mix_hbm, wa_hbm, wp_hbm)
+    targets = (dl_ref, rl_ref, wk_ref, wr_ref, wv_ref, wi_ref, mix_ref, wa_ref, wp_ref)
+    loads = [
+        pltpu.make_async_copy(source, target, loaded.at[i])
+        for i, (source, target) in enumerate(zip(sources, targets))
+    ]
+    for load in loads:
+        load.start()
+    front_part(
+        nfs,
+        x_ref,
+        in_gain_ref,
+        (wk_ref, wr_ref, wv_ref, wi_ref),
+        (dl_ref, rl_ref),
+        loads[:6],
+        pool_ref,
+        lat_ref,
+        mine,
+        cells,
+        part,
+        pool_part,
+        landed,
+        pool_landed,
+        xs,
+        xr,
+        ps,
+        pr,
+        count,
+        lambda pair, lanes, key, receptance, value: mix_pair(
+            pair,
+            lanes,
+            key,
+            receptance,
+            value,
+            lat_ref,
+            draise_ref,
+            dbias_ref,
+            rraise_ref,
+            rbias_ref,
+            tempo_ref,
+            extra_ref,
+            query_ref,
+            local_ref,
+            transfer_ref,
+            carried_ref,
+        ),
+    )
+    for load in loads[6:]:
+        load.wait()
+    edge[0] = pool_ref[:HALO]
+    edge[1] = pool_ref[tokens - HALO :]
 
     sides = [(has_prev, prev, has_next), (has_next, after, has_prev)]
-    state_copies = [
-        remote(leaving.at[0], incoming.at[0], ss.at[0], sr.at[0], "sp", after),
-        remote(leaving.at[1], incoming.at[1], ss.at[1], sr.at[1], "sp", prev),
-    ]
+    def state_copy(d, p):
+        return remote(
+            leaving.at[d, p],
+            incoming.at[d, p],
+            ss.at[d, p],
+            sr.at[d, p],
+            "sp",
+            after if d == 0 else prev,
+        )
+
     halo_copies = [
         remote(edge.at[1], halo.at[0], hs.at[0], hr.at[0], "sp", after),
         remote(edge.at[0], halo.at[1], hs.at[1], hr.at[1], "sp", prev),
@@ -351,22 +476,22 @@
     takes = [has_prev, has_next]
 
     def relay(d):
-        @pl.when(takes[d])
-        def _():
-            state_copies[d].wait_recv()
-
         @pl.when(jnp.logical_not(takes[d]))
         def _():
             incoming[d] = jnp.zeros_like(incoming[d])
 
-        @pl.when(sends[d])
-        def _():
-            for p in range(pairs):
-                rows = slice(p * HEAD, (p + 1) * HEAD)
-                leaving[d, rows] = (
-                    dot(incoming[d, rows], transfer_ref[d, p]) + carried_ref[d, p]
+        for p in range(pairs):
+
+            @pl.when(takes[d])
+            def _():
+                state_copy(d, p).wait_recv()
+
+            @pl.when(sends[d])
+            def _():
+                leaving[d, p] = (
+                    dot(incoming[d, p], transfer_ref[d, p]) + carried_ref[d, p]
                 ).astype(bf16)
-            state_copies[d].start()
+                state_copy(d, p).start()
 
     def start_halo(d):
         pl.when(sends[d])(lambda: halo_copies[d].start())
@@ -394,7 +519,7 @@
             halo[d] = jnp.zeros_like(halo[d])
 
     span = tokens + 2 * HALO
-    rim = jnp.concatenate([halo[0], p4_ref[3], halo[1]], 0)
+    rim = jnp.concatenate([halo[0], pool_ref[...], halo[1]], 0)
     here = lax.broadcasted_iota(jnp.int32, (tokens, span), 0)
     there = lax.broadcasted_iota(jnp.int32, (tokens, span), 1) - HALO
     position = z * tokens + lax.broadcasted_iota(jnp.int32, (tokens, GROUP_WIDTH), 0)
@@ -408,7 +533,7 @@
         size = (
             jnp.minimum(position + reach, length) - jnp.maximum(position - reach, 0)
         ).astype(f32)
-        diff = (total / size - p4_ref[3, :, cols].astype(f32)).astype(bf16)
+        diff = (total / size - pool_ref[:, cols].astype(f32)).astype(bf16)
         act[me, 0, :, cols] = dot(diff, mix_ref[member]).astype(bf16)
     order = [nfs // 2] + [d for d in range(1, nfs) if d != nfs // 2]
     shares = []
@@ -432,7 +557,7 @@
         lanes = slice(p * LANES, (p + 1) * LANES)
         readout = local_ref[:, lanes]
         for d in range(2):
-            state = incoming[d, p * HEAD : (p + 1) * HEAD].astype(f32)
+            state = incoming[d, p].astype(f32)
             wide = jnp.concatenate(
                 [jnp.where(top0, state, 0.0), jnp.where(top0, 0.0, state)], 0
             )
@@ -492,7 +617,8 @@
 
         @pl.when(sends[d])
         def _():
-            state_copies[d].wait_send()
+            for p in range(pairs):
+                state_copy(d, p).wait_send()
             halo_copies[d].wait_send()
 
 
@@ -520,104 +646,56 @@
     _, tokens, features = inputs.shape
     depth, channels = key_matrix.shape
     pairs = channels // LANES
-    heads = channels // HEAD
     dma = pltpu.SemaphoreType.DMA
-    limit = 60 * 1024 * 1024
-    p4, lat = pl.pallas_call(
-        functools.partial(front_kernel, nfs),
-        out_shape=(
-            jax.ShapeDtypeStruct((4, tokens, channels), bf16),
-            jax.ShapeDtypeStruct((2, tokens, decay_lower_matrix.shape[1]), bf16),
-        ),
-        in_specs=[VMEM] * 8,
-        out_specs=(VMEM, VMEM),
-        scratch_shapes=[
+    rank = decay_lower_matrix.shape[1]
+    rank2 = decay_raise_matrix.shape[0] * decay_raise_matrix.shape[1]
+    anywhere = pl.BlockSpec(memory_space=pl.ANY)
+    half = (nfs, tokens // ntp, depth)
+    return pl.pallas_call(
+        functools.partial(layer_kernel, nsp, nfs, ntp),
+        out_shape=jax.ShapeDtypeStruct((1, tokens // ntp, features), bf16),
+        in_specs=[VMEM] * 2
+        + [anywhere] * 6
+        + [VMEM] * 6
+        + [anywhere, VMEM, anywhere, anywhere],
+        out_specs=VMEM,
+        scratch_shapes=[pltpu.VMEM((depth, channels), bf16)] * 4
+        + [
+            pltpu.VMEM((features, rank), bf16),
+            pltpu.VMEM((features, rank), bf16),
+            pltpu.VMEM(group_mixing_weight.shape, bf16),
+            pltpu.VMEM(attention_output_matrix.shape, bf16),
+            pltpu.VMEM(pooling_output_matrix.shape, bf16),
+            dma((9,)),
             pltpu.VMEM((nfs, tokens, depth), bf16),
             pltpu.VMEM((nfs, tokens, depth), bf16),
-            pltpu.VMEM((nfs, 4, tokens, channels), bf16),
-            pltpu.VMEM((nfs, 4, tokens, channels), bf16),
+            pltpu.VMEM((nfs, pairs, 3, tokens, LANES), bf16),
+            pltpu.VMEM((nfs, tokens, channels), bf16),
+            pltpu.VMEM((nfs, pairs, 3, tokens, LANES), bf16),
+            pltpu.VMEM((nfs, tokens, channels), bf16),
             dma((nfs,)),
             dma((nfs,)),
-            dma((nfs, 4)),
-            dma((nfs, 4)),
-        ],
-        compiler_params=pltpu.CompilerParams(
-            collective_id=0, has_side_effects=True, vmem_limit_bytes=limit
-        ),
-        name="front",
-    )(
-        inputs,
-        input_norm_gain[None],
-        receptance_matrix,
-        key_matrix,
-        value_matrix,
-        pooling_input_weight,
-        decay_lower_matrix,
-        removal_lower_matrix,
-    )
-
-    def whole(*shape):
-        return pl.BlockSpec(shape, lambda p: (0,) * len(shape))
-
-    rank2 = decay_raise_matrix.shape[0] * decay_raise_matrix.shape[1]
-    query, local, transfer, carried = pl.pallas_call(
-        mixer_kernel,
-        grid=(pairs,),
-        out_shape=(
-            jax.ShapeDtypeStruct((2, tokens, channels), bf16),
-            jax.ShapeDtypeStruct((tokens, channels), f32),
-            jax.ShapeDtypeStruct((2, pairs, LANES, LANES), f32),
-            jax.ShapeDtypeStruct((2, pairs, HEAD, LANES), f32),
-        ),
-        in_specs=[
-            pl.BlockSpec((4, tokens, LANES), lambda p: (0, 0, p)),
-            whole(2, tokens, decay_lower_matrix.shape[1]),
-            pl.BlockSpec((rank2, LANES), lambda p: (0, p)),
-            pl.BlockSpec((2, LANES), lambda p: (0, p)),
-            pl.BlockSpec((rank2, LANES), lambda p: (0, p)),
-            pl.BlockSpec((2, LANES), lambda p: (0, p)),
-            whole(2, heads, tokens),
-            whole(2, heads, tokens),
-        ],
-        out_specs=(
-            pl.BlockSpec((2, tokens, LANES), lambda p: (0, 0, p)),
-            pl.BlockSpec((tokens, LANES), lambda p: (0, p)),
-            pl.BlockSpec((2, 1, LANES, LANES), lambda p: (0, p, 0, 0)),
-            pl.BlockSpec((2, 1, HEAD, LANES), lambda p: (0, p, 0, 0)),
-        ),
-        compiler_params=pltpu.CompilerParams(
-            vmem_limit_bytes=limit, dimension_semantics=("arbitrary",)
-        ),
-        name="mixer",
-    )(
-        p4,
-        lat,
-        decay_raise_matrix.reshape(rank2, channels),
-        decay_offset_bias,
-        removal_raise_matrix.reshape(rank2, channels),
-        removal_rate_bias,
-        tempo_scale[0],
-        sudden_decay_extra[0],
-    )
-    return pl.pallas_call(
-        functools.partial(tail_kernel, nsp, nfs, ntp),
-        out_shape=jax.ShapeDtypeStruct((1, tokens // ntp, features), bf16),
-        in_specs=[VMEM] * 9,
-        out_specs=VMEM,
-        scratch_shapes=[
+            dma((nfs, pairs + 1)),
+            dma((nfs, pairs + 1)),
+            pltpu.VMEM((2, tokens, rank), bf16),
+            pltpu.VMEM((tokens, channels), bf16),
+            pltpu.VMEM((2, tokens, channels), bf16),
+            pltpu.VMEM((tokens, channels), f32),
+            pltpu.VMEM((2, pairs, LANES, LANES), f32),
+            pltpu.VMEM((2, pairs, HEAD, LANES), f32),
             pltpu.VMEM((2, HALO, channels), bf16),
             pltpu.VMEM((2, HALO, channels), bf16),
-            pltpu.VMEM((2, pairs * HEAD, LANES), bf16),
-            pltpu.VMEM((2, pairs * HEAD, LANES), bf16),
+            pltpu.VMEM((2, pairs, HEAD, LANES), bf16),
+            pltpu.VMEM((2, pairs, HEAD, LANES), bf16),
             pltpu.VMEM((nfs, 2, tokens, channels), bf16),
-            pltpu.VMEM((nfs, tokens // ntp, depth), bf16),
-            pltpu.VMEM((nfs, tokens // ntp, depth), bf16),
-            pltpu.VMEM((nfs, tokens // ntp, depth), bf16),
-            pltpu.VMEM((nfs, tokens // ntp, depth), bf16),
+            pltpu.VMEM(half, bf16),
+            pltpu.VMEM(half, bf16),
+            pltpu.VMEM(half, bf16),
+            pltpu.VMEM(half, bf16),
             dma((2,)),
             dma((2,)),
-            dma((2,)),
-            dma((2,)),
+            dma((2, pairs)),
+            dma((2, pairs)),
             dma((nfs, 2)),
             dma((nfs, 2)),
             dma((nfs,)),
@@ -626,15 +704,24 @@
             dma((nfs,)),
         ],
         compiler_params=pltpu.CompilerParams(
-            collective_id=1, has_side_effects=True, vmem_limit_bytes=limit
+            collective_id=0, has_side_effects=True, vmem_limit_bytes=60 * 1024 * 1024
         ),
-        name="tail",
+        name="layer",
     )(
-        query,
-        local,
-        transfer,
-        carried,
-        p4,
+        inputs,
+        input_norm_gain[None],
+        key_matrix,
+        receptance_matrix,
+        value_matrix,
+        pooling_input_weight,
+        decay_lower_matrix,
+        removal_lower_matrix,
+        decay_raise_matrix.reshape(rank2, channels),
+        decay_offset_bias,
+        removal_raise_matrix.reshape(rank2, channels),
+        removal_rate_bias,
+        tempo_scale[0],
+        sudden_decay_extra[0],
         group_mixing_weight,
         head_norm_gain[None],
         attention_output_matrix,

time: 90.4 us -> 67.7 us (0.75)
  Pallas kernels: 86.6 us -> 64 us
    pallas_call x3 -> x1, Pallas kernels: 86.6 us -> 64 us  [shards(): pl.pallas_call(functools.partial(layer_kernel, nsp, nfs, ntp), out_shape=...]
where the time goes in v1:
time: 67.7 us; the launch traced here: 67.5 us
  Pallas kernels  64 us (95%)
  local copies, waits for them, and re-layouts  3.57 us (5%)
    pallas_call x1, Pallas kernels, shards(): pl.pallas_call(functools.partial(layer_kernel, nsp, nfs, ntp), out_shape=...  64 us
    unnamed x5, local copies, waits for them, and re-layouts  2.37 us

profile of v1, /device:TPU:0, one launch (start us, length us, event | category | flops | bytes accessed | tf_op | source)
XLA Modules:
  0.0 67.5 jit_solution(5244314185638613739)
XLA Ops:
  0.0 0.0 copy-start
  0.0 0.0 copy-start.1
  0.0 0.7 %copy-done.1 = bf16[512]{0:T(512)(128)(2,1)S(1)} copy-done((bf16[512]{0:T(512)(128)(2,1)S(1)}, bf16[512]{0:T(512)(128)(2,1)}, u32[]{:S(2)}) %copy-start.1) | copy-done | bytes 1048
  0.7 0.6 broadcast_in_dim.7.gain_ref
  1.3 0.0 copy-done
  1.3 0.6 broadcast_in_dim.6.in_gain_ref
  1.9 64.0 %layer.1 = bf16[1,64,2048]{2,1,0:T(8,128)(2,1)} custom-call(bf16[1,128,2048]{2,1,0:T(8,128)(2,1)} %x_ref.1, bf16[1,2048]{1,0:T(2,128)(2,1)} %broadcast_in_dim.6.in_gain_ref, bf16[512,512]{1,0:T(8,128)(2,1)} %wk_hbm.1, bf16[512,512]{1,0:T(8,128)(2,1)} %wr_hbm.1, bf16[512,512]{1,0:T(8,128)(2,1)} %wv_hbm.1, bf16[512,512]{1,0:T(8,128)(2,1)} %wi_hbm.1, ...), custom_call_target="tpu_custom_call" | custom-call | tf_op jit(solution)/shard_map/layer/pallas_call | solution.py:654
  65.9 1.7 %copy.20 = bf16[1,64,2048]{2,1,0:T(8,128)(2,1)} copy(bf16[1,64,2048]{2,1,0:T(8,128)(2,1)} %layer.1) | data formatting | bytes 524288
Async XLA Ops:
  0.0 1.3 %copy-start = (bf16[2048]{0:T(1024)(128)(2,1)S(1)}, bf16[2048]{0:T(1024)(128)(2,1)}, u32[]{:S(2)}) copy-start(bf16[2048]{0:T(1024)(128)(2,1)} %param.19) | copy-start | bytes 12292
  0.0 0.7 %copy-start.1 = (bf16[512]{0:T(512)(128)(2,1)S(1)}, bf16[512]{0:T(512)(128)(2,1)}, u32[]{:S(2)}) copy-start(bf16[512]{0:T(512)(128)(2,1)} %param.32) | copy-start | bytes 3076

commit v2 on v1

--- a/solution.py
+++ b/solution.py
@@ -60,6 +60,16 @@
     pl.semaphore_signal(
         barrier, inc=1, device_id={axis: peer}, device_id_type=pl.DeviceIdType.MESH
     )
+
+
+def flipped(at, bits):
+    moved = at
+    bit = 1
+    while bit <= bits:
+        if bits & bit:
+            moved = moved + bit - 2 * bit * lax.rem(at // bit, 2)
+        bit *= 2
+    return moved
 
 
 def front_part(
@@ -85,25 +95,30 @@
     mix_pair,
 ):
     me = lax.axis_index("fs")
+    core, ntp = lax.axis_index("tp"), lax.axis_size("tp")
     width = x_ref.shape[2] // n
+    share = x_ref.shape[1] // ntp
+    rows = pl.ds(pl.multiple_of(core * share, share), share)
     pairs = part.shape[1]
     x = x_ref[0].astype(f32)
     normed = (
         x
         * lax.rsqrt(jnp.mean(x * x, axis=-1, keepdims=True) + norm_eps)
-        * gain_ref[...].astype(f32)
+        * gain_ref[...].astype(f32).reshape(1, -1)
     ).astype(bf16)
     for j in range(n):
         mine[j] = normed[:, j * width : (j + 1) * width]
     pl.semaphore_wait(pltpu.get_barrier_semaphore(), count)
-    order = [n // 2] + [d for d in range(1, n) if d != n // 2]
+    order = list(range(n - 1, 0, -1))
     moves = []
     for d in order:
-        peer = lax.rem(me + d, n)
-        copy = remote(mine.at[peer], cells.at[me], xs.at[d], xr.at[d], "fs", peer)
+        peer = flipped(me, d)
+        copy = remote(
+            mine.at[peer, rows], cells.at[me, rows], xs.at[d, 0], xr.at[d, 0], "fs", peer
+        )
         copy.start()
         moves.append(copy)
-    for load in loads:
+    for load in loads[:2]:
         load.wait()
     dl_ref, rl_ref = lowers
     decay = jnp.zeros((x.shape[0], dl_ref.shape[1]), f32)
@@ -114,17 +129,33 @@
         rate = rate + dot(block, rl_ref[j * width : (j + 1) * width])
     lat_ref[0] = jnp.tanh(decay.astype(bf16).astype(f32)).astype(bf16)
     lat_ref[1] = rate.astype(bf16)
-    for copy in moves:
+    for load in loads[2:]:
+        load.wait()
+    for d, copy in zip(order, list(moves)):
+        peer = flipped(me, d)
         copy.wait_recv()
+        for e in range(1, ntp):
+            passed = remote(
+                cells.at[peer, rows],
+                cells.at[peer, rows],
+                xs.at[d, e],
+                xr.at[d, e],
+                "tp",
+                lax.rem(core + e, ntp),
+            )
+            passed.start()
+            moves.append(passed)
+    for copy in moves[len(order) :]:
+        copy.wait_recv()
 
     def pair_copy(d, p):
-        peer = lax.rem(me + d, n)
+        peer = flipped(me, d)
         return remote(
             part.at[peer, p], landed.at[me, p], ps.at[d, p], pr.at[d, p], "fs", peer
         )
 
     def pool_copy(d):
-        peer = lax.rem(me + d, n)
+        peer = flipped(me, d)
         return remote(
             pool_part.at[peer],
             pool_landed.at[me],
@@ -136,14 +167,14 @@
 
     for p in range(pairs):
         for d in order:
-            peer = lax.rem(me + d, n)
+            peer = flipped(me, d)
             for m in range(3):
                 part[peer, p, m] = dot(
                     cells[peer], weights[m][:, p * LANES : (p + 1) * LANES]
                 ).astype(bf16)
             pair_copy(d, p).start()
     for d in order:
-        peer = lax.rem(me + d, n)
+        peer = flipped(me, d)
         pool_part[peer] = dot(cells[peer], weights[3][...]).astype(bf16)
         pool_copy(d).start()
 
@@ -153,7 +184,7 @@
         for d in range(1, n):
             pair_copy(d, p).wait_recv()
         for d in range(1, n):
-            peer = lax.rem(me + d, n)
+            peer = flipped(me, d)
             owned = [o + landed[peer, p, m].astype(f32) for m, o in enumerate(owned)]
         mix_pair(p, lanes, *[o.astype(bf16) for o in owned])
         return carry
@@ -163,7 +194,7 @@
     for d in range(1, n):
         pool_copy(d).wait_recv()
     for d in range(1, n):
-        total = total + pool_landed[lax.rem(me + d, n)].astype(f32)
+        total = total + pool_landed[flipped(me, d)].astype(f32)
     pool_ref[...] = total.astype(bf16)
     for copy in moves:
         copy.wait_send()
@@ -399,7 +430,7 @@
 
     barrier = pltpu.get_barrier_semaphore()
     for d in range(1, nfs):
-        greet(barrier, "fs", lax.rem(me + d, nfs))
+        greet(barrier, "fs", flipped(me, d))
     for d in range(1, ntp):
         greet(barrier, "tp", lax.rem(core + d, ntp))
     pl.when(has_prev)(lambda: greet(barrier, "sp", prev))
@@ -535,10 +566,10 @@
         ).astype(f32)
         diff = (total / size - pool_ref[:, cols].astype(f32)).astype(bf16)
         act[me, 0, :, cols] = dot(diff, mix_ref[member]).astype(bf16)
-    order = [nfs // 2] + [d for d in range(1, nfs) if d != nfs // 2]
+    order = list(range(nfs - 1, 0, -1))
     shares = []
     for d in order:
-        peer = lax.rem(me + d, nfs)
+        peer = flipped(me, d)
         copy = remote(act.at[me, 0], act.at[me, 0], gs.at[d, 0], gr.at[d, 0], "fs", peer)
         copy.start()
         shares.append(copy)
@@ -570,12 +601,21 @@
 
         centred = readout - head_mean(readout)
         scaled = centred * lax.rsqrt(head_mean(centred * centred) + head_eps)
-        act[me, 1, :, lanes] = (scaled * gain_ref[:, lanes].astype(f32)).astype(bf16)
-    for d in order:
-        peer = lax.rem(me + d, nfs)
-        copy = remote(act.at[me, 1], act.at[me, 1], gs.at[d, 1], gr.at[d, 1], "fs", peer)
-        copy.start()
-        shares.append(copy)
+        act[me, 1, :, lanes] = (scaled * gain_ref[lanes].astype(f32).reshape(1, -1)).astype(bf16)
+        if (p + 1) % (pairs // 2) == 0:
+            part = (p + 1) // (pairs // 2)
+            cols = pl.ds((part - 1) * (channels // 2), channels // 2)
+            for d in order:
+                copy = remote(
+                    act.at[me, 1, :, cols],
+                    act.at[me, 1, :, cols],
+                    gs.at[d, part],
+                    gr.at[d, part],
+                    "fs",
+                    flipped(me, d),
+                )
+                copy.start()
+                shares.append(copy)
 
     other = lax.rem(core + 1, ntp)
     mine_at = pl.multiple_of(core * half_rows, half_rows)
@@ -586,11 +626,11 @@
 
     returns = []
     swaps = []
-    turns = [0] + [d for d in range(1, nfs) if d != nfs // 2] + [nfs // 2]
+    turns = [0] + order
     for d in turns:
-        seq = lax.rem(me + nfs - d, nfs)
+        seq = flipped(me, d)
         if d:
-            for copy, at in zip(shares, order + order):
+            for copy, at in zip(shares, order * 3):
                 if at == d:
                     copy.wait_recv()
         tsend[d] = product(seq, pl.ds(other_at, half_rows)).astype(bf16)
@@ -673,8 +713,8 @@
             pltpu.VMEM((nfs, tokens, channels), bf16),
             pltpu.VMEM((nfs, pairs, 3, tokens, LANES), bf16),
             pltpu.VMEM((nfs, tokens, channels), bf16),
-            dma((nfs,)),
-            dma((nfs,)),
+            dma((nfs, ntp)),
+            dma((nfs, ntp)),
             dma((nfs, pairs + 1)),
             dma((nfs, pairs + 1)),
             pltpu.VMEM((2, tokens, rank), bf16),
@@ -696,8 +736,8 @@
             dma((2,)),
             dma((2, pairs)),
             dma((2, pairs)),
-            dma((nfs, 2)),
-            dma((nfs, 2)),
+            dma((nfs, 3)),
+            dma((nfs, 3)),
             dma((nfs,)),
             dma((nfs,)),
             dma((nfs,)),
@@ -709,7 +749,7 @@
         name="layer",
     )(
         inputs,
-        input_norm_gain[None],
+        input_norm_gain,
         key_matrix,
         receptance_matrix,
         value_matrix,
@@ -723,7 +763,7 @@
         tempo_scale[0],
         sudden_decay_extra[0],
         group_mixing_weight,
-        head_norm_gain[None],
+        head_norm_gain,
         attention_output_matrix,
         pooling_output_matrix,
     )

time: 67.7 us -> 64.9 us (0.959)
  local copies, waits for them, and re-layouts: 3.57 us -> 1.67 us
  Pallas kernels: 64 us -> 63.1 us
    broadcast_in_dim x2 -> x0, local copies, waits for them, and re-layouts: 1.2 us -> none  [the longest x1 0.6 us: shards(): input_norm_gain[None]]
    pallas_call x1, Pallas kernels: 64 us -> 63.1 us  [shards(): pl.pallas_call(functools.partial(layer_kernel, nsp, nfs, ntp), out_shape=...]
    unnamed x5 -> x1, local copies, waits for them, and re-layouts: 2.37 us -> 1.67 us
where the time goes in v2:
time: 64.9 us; the launch traced here: 64.8 us
  Pallas kernels  63.1 us (97%)
  local copies, waits for them, and re-layouts  1.67 us (3%)
    pallas_call x1, Pallas kernels, shards(): pl.pallas_call(functools.partial(layer_kernel, nsp, nfs, ntp), out_shape=...  63.1 us
    unnamed x1, local copies, waits for them, and re-layouts  1.67 us

profile of v2, /device:TPU:0, one launch (start us, length us, event | category | flops | bytes accessed | tf_op | source)
XLA Modules:
  0.0 64.8 jit_solution(16902383792678042496)
XLA Ops:
  0.0 63.1 %layer.1 = bf16[1,64,2048]{2,1,0:T(8,128)(2,1)} custom-call(bf16[1,128,2048]{2,1,0:T(8,128)(2,1)} %x_ref.1, bf16[2048]{0:T(1024)(128)(2,1)} %in_gain_ref.1, bf16[512,512]{1,0:T(8,128)(2,1)} %wk_hbm.1, bf16[512,512]{1,0:T(8,128)(2,1)} %wr_hbm.1, bf16[512,512]{1,0:T(8,128)(2,1)} %wv_hbm.1, bf16[512,512]{1,0:T(8,128)(2,1)} %wi_hbm.1, bf16[2048,128]{1,0:T(8,128)(2,1)} %dl_hbm.1, ...), custom_call_target="tpu_custom_call" | custom-call | tf_op jit(solution)/shard_map/layer/pallas_call | solution.py:694
  63.1 1.7 %copy.20 = bf16[1,64,2048]{2,1,0:T(8,128)(2,1)} copy(bf16[1,64,2048]{2,1,0:T(8,128)(2,1)} %layer.1) | data formatting | bytes 524288

commit v3 on v2

--- a/solution.py
+++ b/solution.py
@@ -39,10 +39,11 @@
     return dot_general(left, right, ((0,), (0,)))
 
 
-def exact_dot(left, right, dims):
-    return lax.dot_general(
-        left, right, (dims, ((), ())), preferred_element_type=f32, precision=lax.Precision.HIGHEST
-    )
+def pieces(cells):
+    high = cells.astype(bf16).astype(f32)
+    rest = cells - high
+    middle = rest.astype(bf16).astype(f32)
+    return jnp.concatenate([high, middle, rest - middle], 0)
 
 
 def remote(src, dst, send, recv, axis, peer):
@@ -237,6 +238,7 @@
         lax.broadcasted_iota(jnp.int32, (heads, LANES), 0)
         == 2 * pair + lax.broadcasted_iota(jnp.int32, (heads, LANES), 1) // HEAD
     ).astype(f32)
+    spread = jnp.concatenate([spread, spread, spread], 0)
     blocks = tokens // BLOCK
     zero_row = jnp.zeros((1, LANES), f32)
     eye = (row == lane).astype(f32)
@@ -256,14 +258,15 @@
         lat_r = jnp.where(lat_mask, lat_ref[1].astype(f32), 0.0)
         pre = dbias_ref[d : d + 1, lanes] + dot(lat_d, draise_ref[:, lanes])
         velocity = jax.nn.sigmoid(pre) * 0.6065306597126334
-        tempo = exact_dot(tempo_ref[d], spread, ((0,), (0,)))
-        extra = exact_dot(extra_ref[d], spread, ((0,), (0,)))
+        tempo = dot_cols(pieces(tempo_ref[d]), spread)
+        extra = dot_cols(pieces(extra_ref[d]), spread)
         ld = -velocity * tempo + extra
         rate = jax.nn.sigmoid(rbias_ref[d : d + 1, lanes] + dot(lat_r, rraise_ref[:, lanes]))
         removal = unit * rate
         written = kf * rate
         upto = (lane <= row) if d == 0 else (lane >= row)
-        inner = exact_dot(upto.astype(f32), ld, ((1,), (0,)))
+        ones = upto.astype(f32)
+        inner = dot(jnp.concatenate([ones, ones, ones], 1), pieces(ld))
         excl = inner - ld
         grams = []
         for i in range(blocks):

time: 64.9 us -> 64.9 us (level)
  no operation moved by 1% of the time
where the time goes in v3:
time: 64.9 us; the launch traced here: 64.8 us
  Pallas kernels  63.1 us (97%)
  local copies, waits for them, and re-layouts  1.67 us (3%)
    pallas_call x1, Pallas kernels, shards(): pl.pallas_call(functools.partial(layer_kernel, nsp, nfs, ntp), out_shape=...  63.1 us
    unnamed x1, local copies, waits for them, and re-layouts  1.67 us

profile of v3, /device:TPU:0, one launch (start us, length us, event | category | flops | bytes accessed | tf_op | source)
XLA Modules:
  0.0 64.8 jit_solution(14490995790180895983)
XLA Ops:
  0.0 63.1 %layer.1 = bf16[1,64,2048]{2,1,0:T(8,128)(2,1)} custom-call(bf16[1,128,2048]{2,1,0:T(8,128)(2,1)} %x_ref.1, bf16[2048]{0:T(1024)(128)(2,1)} %in_gain_ref.1, bf16[512,512]{1,0:T(8,128)(2,1)} %wk_hbm.1, bf16[512,512]{1,0:T(8,128)(2,1)} %wr_hbm.1, bf16[512,512]{1,0:T(8,128)(2,1)} %wv_hbm.1, bf16[512,512]{1,0:T(8,128)(2,1)} %wi_hbm.1, bf16[2048,128]{1,0:T(8,128)(2,1)} %dl_hbm.1, ...), custom_call_target="tpu_custom_call" | custom-call | tf_op jit(solution)/shard_map/layer/pallas_call | solution.py:697
  63.1 1.7 %copy.20 = bf16[1,64,2048]{2,1,0:T(8,128)(2,1)} copy(bf16[1,64,2048]{2,1,0:T(8,128)(2,1)} %layer.1) | data formatting | bytes 524288
